TPU v7x, 32 devices: a whole 2x2x4 slice. The times are simulated.
32 devices in a mesh: sp: 8 (over z, y), tp: 4 (over x, core).
Axes of the slice: x: 2, y: 2, z: 4, core: 2. Of those that a mesh axis runs over, the one named last changes fastest.
Arguments:
- conv_outer: bfloat16 [6144, 2048], P('sp', 'tp'), may hold values from -6 to 6
- conv_inner: bfloat16 [6144, 2048], P('sp', 'tp'), may hold values from -6 to 6
- conv_input: bfloat16 [6144, 2048], P('sp', 'tp'), may hold values from -6 to 6
- conv_taps: float32 [3, 2048], P(None, 'tp'), may hold values from -3.5 to 3.5
- out_weight: bfloat16 [2048, 2048], P('tp'), may hold values from -0.125 to 0.125
- mix_gate: bfloat16 [6144, 2048], P(('sp', 'tp')), may hold values from -8 to 8
- residual: bfloat16 [6144, 2048], P(('sp', 'tp')), may hold values from -6 to 6
- mix_gain: float32 [2048], replicated, may hold values from 0.1 to 1.9
- expert_gain: float32 [2048], replicated, may hold values from 0.1 to 1.9
- expert_ids: int32 [6144, 2], P(('sp', 'tp')), may hold values from 0 to 7, all different within a row; in each aligned block of 192 rows (0 to 191, 192 to 383, ...) at most 96 rows name the same one
- group_share: float32 [6144], P(('sp', 'tp')), may hold values from 0.25 to 1
- pair_scores: float32 [6144, 2], P(('sp', 'tp')), may hold values from -8 to 8
- gate_experts: bfloat16 [8, 2048, 512], P('sp'), may hold values from -0.125 to 0.125
- up_experts: bfloat16 [8, 2048, 512], P('sp'), may hold values from -0.125 to 0.125
- down_experts: bfloat16 [8, 512, 2048], P('sp'), may hold values from -0.25 to 0.25
Outputs:
- layer_out: bfloat16 [6144, 2048], P(('sp', 'tp'))
Inputs may be any that keep to these rules, and one draw needn't show every extreme that they name: `expert_ids`: within the rows of one device (aligned blocks of 192 rows), no expert is named by more than 96 rows, a bound that some block reaches; the 2 experts of a row differ.
All inputs are finite; a program needn't handle non-finite values.
Results may differ from a plain program's by a relative error of at most 0.0069.
Values may be sent and summed in bfloat16 or wider, within the bound.
A program may use at most 128 MiB of HBM per device.

v0:
```python
import jax
import jax.numpy as jnp
from jax import lax
from jax.sharding import PartitionSpec as P

epsilon = 1e-06


def f32(value):
    return value.astype(jnp.float32)


def bf16(value):
    return value.astype(jnp.bfloat16)


def rms_scale(values, gain):
    return values * lax.rsqrt(jnp.mean(values * values, axis=-1, keepdims=True) + epsilon) * gain


def shifted(value, steps, senders):
    return lax.ppermute(value, "sp", [(s, s + steps) for s in senders])


def swapped(value, axis, bit):
    return lax.ppermute(value, axis, [(s, s ^ bit) for s in range(lax.axis_size(axis))])


def mixer_rows(conv_outer, conv_inner, conv_input, conv_taps):
    kept = conv_taps.shape[0] - 1
    inner = f32(conv_inner) * f32(conv_input)
    tail = f32(conv_inner[-kept:]) * f32(conv_input[-kept:])
    earlier = shifted(tail, 1, range(lax.axis_size("sp") - 1))
    length = conv_inner.shape[0]
    inner = jnp.concatenate([earlier, inner], 0)
    conv = conv_taps[0] * inner[0:length]
    for offset in range(1, kept + 1):
        conv = conv + conv_taps[offset] * inner[offset : offset + length]
    return bf16(f32(conv_outer) * conv)


def project(mixed_rows, out_weight, own_rows):
    parts = lax.axis_size("tp")
    me = lax.axis_index("tp")
    blocks = mixed_rows.reshape(parts, own_rows, -1)

    def partial(owner):
        rows = lax.dynamic_index_in_dim(blocks, owner, 0, keepdims=False)
        return jnp.dot(rows, out_weight, preferred_element_type=jnp.float32)

    def total(owner_bits, bit):
        if bit == 1:
            return partial(me ^ owner_bits)
        half = bit // 2
        given = swapped(bf16(total(owner_bits | half, half)), "tp", half)
        return total(owner_bits, half) + f32(given)

    return total(0, parts)


def per_device(
    conv_outer,
    conv_inner,
    conv_input,
    conv_taps,
    out_weight,
    mix_gate,
    residual,
    mix_gain,
    expert_gain,
    expert_ids,
    group_share,
    pair_scores,
    gate_experts,
    up_experts,
    down_experts,
):
    count = lax.axis_size("sp")
    me = lax.axis_index("sp")
    own_rows = residual.shape[0]
    groups = count // 2
    place = me // 2
    side = lax.axis_index("tp") % 2
    half = gate_experts.shape[2] // 2

    def fetched(weight, axis):
        piece = lax.dynamic_slice_in_dim(weight[0], side * half, half, axis)
        first = swapped(piece, "sp", 1)
        second = swapped(first, "tp", 1)
        return jnp.concatenate([weight[0], first, second], axis)

    gate_both = fetched(gate_experts, 1)
    up_both = fetched(up_experts, 1)
    down_both = fetched(down_experts, 0)

    weights = group_share[:, None] * jax.nn.softmax(pair_scores, axis=-1)
    lanes = -(-2 * count // 128) * 128
    column = jnp.arange(lanes, dtype=jnp.int32)[None, :]
    coarse = lax.reduce_precision(weights, 8, 7)
    fine = weights - coarse
    table = jnp.zeros((own_rows, lanes), jnp.float32)
    for slot in range(expert_ids.shape[1]):
        at = expert_ids[:, slot : slot + 1]
        table = table + jnp.where(column == at, coarse[:, slot : slot + 1], 0.0)
        table = table + jnp.where(column == at + count, fine[:, slot : slot + 1], 0.0)
    table = bf16(table)

    def spread(own):
        below, above = {0: own}, {0: own}
        for step in range(1, groups):
            below[step] = shifted(below[step - 1], 2, range(2 * (step - 1), count - 2))
            above[step] = shifted(above[step - 1], -2, range(2, count - 2 * (step - 1)))
        order = {0: own}
        for near in range(1, (groups - 1) // 2 + 1):
            far = groups - near
            early = jnp.where(place < near, above[near], below[near])
            _, over, under, away = lax.optimization_barrier(
                (early, above[near], below[far], above[far])
            )
            order[near] = early
            late = jnp.where(place < far, over, under)
            order[far] = jnp.where(place < near, away, late)
        if groups % 2 == 0:
            mid = groups // 2
            order[mid] = jnp.where(place < mid, above[mid], below[mid])
        return order

    mixed_rows = mixer_rows(conv_outer, conv_inner, conv_input, conv_taps)
    projected = project(mixed_rows, out_weight, own_rows)
    mixed = jax.nn.sigmoid(f32(mix_gate)) * projected
    hidden_state = bf16(f32(residual) + rms_scale(mixed, mix_gain))
    normed = bf16(rms_scale(f32(hidden_state), expert_gain))

    blocks = spread(jnp.concatenate([normed, table], 1))
    depth = normed.shape[1]

    def served(block):
        rows, shares = block[:, :depth], f32(block[:, depth:])

        def share_of(expert):
            chosen = (column == expert) | (column == expert + count)
            return jnp.sum(jnp.where(chosen, shares, 0.0), axis=1, keepdims=True)

        wide = 2 * half
        first = jnp.dot(rows, gate_both, preferred_element_type=jnp.float32)
        second = jnp.dot(rows, up_both, preferred_element_type=jnp.float32)
        mine = jnp.arange(2 * wide)[None, :] < wide
        share = jnp.where(mine, share_of(me), share_of(me ^ 1))
        hidden = lax.optimization_barrier(bf16(jax.nn.silu(first) * second * share))
        return lax.optimization_barrier(
            jnp.dot(hidden, down_both, preferred_element_type=jnp.float32)
        )

    results = {number: served(block) for number, block in blocks.items()}

    def for_upper(step):
        gone = groups - step
        if step == gone or step < gone:
            return results[gone]
        return jnp.where(place < gone, results[gone], results[step])

    down = up = None
    for step in range(1, groups):
        gone = groups - step
        lower, upper = results[gone], for_upper(step)
        if down is not None:
            lower, upper = lower + f32(down), upper + f32(up)
        down = shifted(bf16(lower), -2, range(2 * gone, count))
        up = shifted(bf16(upper), 2, range(0, count - 2 * gone))
    result = f32(hidden_state) + results[0]
    if down is not None:
        result = result + f32(down) + f32(up)
    return bf16(result)


def solution(mesh):
    placed = (
        P("sp", "tp"),
        P("sp", "tp"),
        P("sp", "tp"),
        P(None, "tp"),
        P("tp", None),
        P(("sp", "tp"), None),
        P(("sp", "tp"), None),
        P(),
        P(),
        P(("sp", "tp"), None),
        P(("sp", "tp")),
        P(("sp", "tp"), None),
        P("sp", None, None),
        P("sp", None, None),
        P("sp", None, None),
    )

    return jax.shard_map(
        per_device, mesh=mesh, in_specs=placed, out_specs=P(("sp", "tp"), None), check_vma=False
    )
```

profile of v0, /device:TPU:0, one launch (start us, length us, event | category | flops | bytes accessed | tf_op | source)
XLA Modules:
  0.0 203.9 jit_solution(8382131809166822375)
XLA Ops:
  0.9 4.9 %collective-permute-start = (f32[2,512]{1,0:T(2,128)S(1)}, f32[2,512]{1,0:T(2,128)S(1)}, u32[]{:S(2)}, u32[]{:S(2)}) collective-permute-start(f32[2,512]{1,0:T(2,128)S(1)} %convert_multiply_fusion.3), channel_id=1, source_target_pairs={{0,4},{4,8},{8,12},{12,16},{16,20},{20,24},{24,28},{1,5},{5,9},{9,... | collective-permute-start | bytes 12296 | tf_op jit(solution)/shard_map/ppermute | solution.py:22
  5.8 2.5 %dynamic-slice_bitcast_fusion.2 = bf16[2048,256]{1,0:T(8,128)(2,1)} fusion(bf16[1,2048,512]{2,1,0:T(8,128)(2,1)} %param.27, s32[]{:T(128)S(6)} %select_n.117), kind=kLoop, calls=%fused_computation.35 | loop fusion | bytes 2097156 | tf_op jit(solution)/shard_map/dynamic_slice | solution.py:87
  15.4 3.6 %fusion.5 = bf16[768,512]{1,0:T(8,128)(2,1)S(1)} fusion(f32[2,512]{1,0:T(2,128)S(1)} %collective-permute-done, f32[768,512]{1,0:T(8,128)} %convert_multiply_fusion.2, bf16[768,512]{1,0:T(8,128)(2,1)} %param.15, f32[512]{0:T(512)S(1)} %bitcast.78, f32[512]{0:T(512)S(1)} %bitcast.79, f32[512]{0:T(512)S(1)} %bitcast.77), kind=kLoop, calls=%fused_computation.15 | loop fusion | flops 3932160 | bytes 3155968 | tf_op jit(solution)/shard_map/convert_element_type | solution.py:14
  23.1 2.6 %add_convert_fusion.5 = bf16[192,2048]{1,0:T(8,128)(2,1)} fusion(bf16[192,2048]{1,0:T(8,128)(2,1)} %collective-permute-done.2, bf16[512,2048]{1,0:T(8,128)(2,1)S(1)} %copy-done, bf16[4,192,512]{2,1,0:T(8,128)(2,1)S(1)} %bitcast.47, s32[]{:T(128)S(6)} %select_n.114), kind=kOutput, calls=%fused_computation.31 | convolution fusion | flops 403832832 | bytes 3866628 | tf_op jit(solution)/shard_map/dot_general | solution.py:49
  28.1 6.5 %collective-permute-done.4 = bf16[2048,256]{1,0:T(8,128)(2,1)} collective-permute-done((bf16[2048,256]{1,0:T(8,128)(2,1)}, bf16[2048,256]{1,0:T(8,128)(2,1)}, u32[]{:S(2)}, u32[]{:S(2)}) %collective-permute-start.4) | collective-permute-done | bytes 1048608 | tf_op jit(solution)/shard_map/ppermute | solution.py:26
  34.6 11.0 %collective-permute-done.3 = bf16[192,2048]{1,0:T(8,128)(2,1)} collective-permute-done((bf16[192,2048]{1,0:T(8,128)(2,1)}, bf16[192,2048]{1,0:T(8,128)(2,1)}, u32[]{:S(2)}, u32[]{:S(2)}) %collective-permute-start.3) | collective-permute-done | bytes 786464 | tf_op jit(solution)/shard_map/ppermute | solution.py:26
  50.5 4.5 %collective-permute-start.11 = (bf16[192,2176]{1,0:T(8,128)(2,1)}, bf16[192,2176]{1,0:T(8,128)(2,1)}, u32[]{:S(2)}, u32[]{:S(2)}) collective-permute-start(bf16[192,2176]{1,0:T(8,128)(2,1)} %pad_maximum_fusion.4), channel_id=1, source_target_pairs={{0,8},{4,12},{8,16},{12,20},{16,24},{20,28},{1,9},{5,13},{9,17},{1... | collective-permute-start | bytes 2506760 | tf_op jit(solution)/shard_map/ppermute | solution.py:22
  57.1 21.1 %collective-permute-done.8 = bf16[256,2048]{1,0:T(8,128)(2,1)} collective-permute-done((bf16[256,2048]{1,0:T(8,128)(2,1)}, bf16[256,2048]{1,0:T(8,128)(2,1)}, u32[]{:S(2)}, u32[]{:S(2)}) %collective-permute-start.8) | collective-permute-done | bytes 1048608 | tf_op jit(solution)/shard_map/ppermute | solution.py:26
  78.2 3.5 %fusion.57 = f32[192,1024]{1,0:T(8,128)S(1)} fusion(bf16[192,2048]{1,0:T(8,128)(2,1)} %copy-done.1, bf16[2048,256]{1,0:T(8,128)(2,1)} %collective-permute-done.5, bf16[2048,256]{1,0:T(8,128)(2,1)} %collective-permute-done.4, bf16[2048,512]{1,0:T(8,128)(2,1)} %bitcast.49), kind=kOutput, calls=%fused_computation.104 | convolution fusion | flops 817889280 | bytes 5767168 | tf_op jit(solution)/shard_map/dot_general | solution.py:145
  85.1 2.9 %fusion.27 = f32[192,1024]{1,0:T(8,128)S(1)} fusion(bf16[192,2176]{1,0:T(8,128)(2,1)S(1)} %broadcast_select_fusion.1, bf16[2048,256]{1,0:T(8,128)(2,1)} %collective-permute-done.5, bf16[2048,256]{1,0:T(8,128)(2,1)} %collective-permute-done.4, bf16[2048,512]{1,0:T(8,128)(2,1)S(1)} %bitcast.50), kind=kOutput, calls=%fused_computation.54 | convolution fusion | flops 817889280 | bytes 5767168 | tf_op jit(solution)/shard_map/dot_general | solution.py:145
  88.7 19.3 %collective-permute-done.12 = bf16[192,2176]{1,0:T(8,128)(2,1)S(1)} collective-permute-done((bf16[192,2176]{1,0:T(8,128)(2,1)}, bf16[192,2176]{1,0:T(8,128)(2,1)S(1)}, u32[]{:S(2)}, u32[]{:S(2)}) %collective-permute-start.12) | collective-permute-done | bytes 835616 | tf_op jit(solution)/shard_map/ppermute | solution.py:22
  109.6 2.9 %fusion.21 = f32[192,1024]{1,0:T(8,128)S(1)} fusion(bf16[192,2176]{1,0:T(8,128)(2,1)S(1)} %broadcast_select_fusion, bf16[2048,256]{1,0:T(8,128)(2,1)} %collective-permute-done.5, bf16[2048,256]{1,0:T(8,128)(2,1)} %collective-permute-done.4, bf16[2048,512]{1,0:T(8,128)(2,1)S(1)} %bitcast.51), kind=kOutput, calls=%fused_computation.50 | convolution fusion | flops 817889280 | bytes 5767168 | tf_op jit(solution)/shard_map/dot_general | solution.py:145
  112.5 17.5 %collective-permute-done.15 = bf16[192,2176]{1,0:T(8,128)(2,1)S(1)} collective-permute-done((bf16[192,2176]{1,0:T(8,128)(2,1)S(1)}, bf16[192,2176]{1,0:T(8,128)(2,1)S(1)}, u32[]{:S(2)}, u32[]{:S(2)}) %collective-permute-start.15) | collective-permute-done | bytes 835616 | tf_op jit(solution)/shard_map/ppermute | solution.py:22
  131.8 3.0 %fusion.15 = f32[192,1024]{1,0:T(8,128)S(1)} fusion(bf16[192,2176]{1,0:T(8,128)(2,1)S(1)} %select_select_fusion, bf16[2048,256]{1,0:T(8,128)(2,1)} %collective-permute-done.5, bf16[2048,256]{1,0:T(8,128)(2,1)} %collective-permute-done.4, bf16[2048,512]{1,0:T(8,128)(2,1)S(1)} %bitcast.52), kind=kOutput, calls=%fused_computation.46 | convolution fusion | flops 817889280 | bytes 5767168 | tf_op jit(solution)/shard_map/dot_general | solution.py:145
  134.9 2.4 %multiply_convert_fusion = bf16[192,1024]{1,0:T(8,128)(2,1)S(1)} fusion(f32[192,1024]{1,0:T(8,128)S(1)} %fusion.15, bf16[192,2176]{1,0:T(8,128)(2,1)S(1)} %select_select_fusion, f32[192]{0:T(256)S(1)} %get-tuple-element.21, f32[192]{0:T(256)S(1)} %get-tuple-element.22, pred[1024]{0:T(1024)(128)(4,1)S(1)} %iota_compare_fusion.4, ...), kind=kOutput, calls=%fused_computation.40 | convolution fusion | flops 819462144 | bytes 6163456 | tf_op jit(solution)/shard_map/dot_general | solution.py:146
  142.0 2.3 %multiply_convert_fusion.1 = bf16[192,1024]{1,0:T(8,128)(2,1)S(1)} fusion(f32[192,1024]{1,0:T(8,128)S(1)} %fusion.21, bf16[192,2176]{1,0:T(8,128)(2,1)S(1)} %broadcast_select_fusion, f32[192]{0:T(256)S(1)} %get-tuple-element.23, f32[192]{0:T(256)S(1)} %get-tuple-element.24, pred[1024]{0:T(1024)(128)(4,1)S(1)} %iota_compare_fusion.4, ...), kind=kOutput, calls=%fused_computation.41 | convolution fusion | flops 819462144 | bytes 6163456 | tf_op jit(solution)/shard_map/dot_general | solution.py:146
  144.2 2.3 %fusion.59 = f32[192,2048]{1,0:T(8,128)S(1)} fusion(bf16[192,1024]{1,0:T(8,128)(2,1)S(1)} %multiply_convert_fusion.1, bf16[256,2048]{1,0:T(8,128)(2,1)S(1)} %collective-permute-done.9, bf16[256,2048]{1,0:T(8,128)(2,1)} %collective-permute-done.8, bf16[512,2048]{1,0:T(8,128)(2,1)S(1)} %bitcast.58), kind=kOutput, calls=%fused_computation.106 | convolution fusion | flops 817889280 | bytes 6160384 | tf_op jit(solution)/shard_map/dot_general | solution.py:151
  146.5 11.2 %collective-permute-done.19 = bf16[192,2048]{1,0:T(8,128)(2,1)S(1)} collective-permute-done((bf16[192,2048]{1,0:T(8,128)(2,1)S(1)}, bf16[192,2048]{1,0:T(8,128)(2,1)S(1)}, u32[]{:S(2)}, u32[]{:S(2)}) %collective-permute-start.19) | collective-permute-done | bytes 786464 | tf_op jit(solution)/shard_map/ppermute | solution.py:22
  159.0 5.0 %collective-permute-start.20 = (bf16[192,2048]{1,0:T(8,128)(2,1)S(1)}, bf16[192,2048]{1,0:T(8,128)(2,1)S(1)}, u32[]{:S(2)}, u32[]{:S(2)}) collective-permute-start(bf16[192,2048]{1,0:T(8,128)(2,1)S(1)} %get-tuple-element.34), channel_id=1, source_target_pairs={{0,8},{4,12},{8,16},{12,20},{1,9},{5,13},{9,17},{13,21},{2,10},{6,... | collective-permute-start | bytes 2359304 | tf_op jit(solution)/shard_map/ppermute | solution.py:22
  168.5 10.4 %collective-permute-done.20 = bf16[192,2048]{1,0:T(8,128)(2,1)S(1)} collective-permute-done((bf16[192,2048]{1,0:T(8,128)(2,1)S(1)}, bf16[192,2048]{1,0:T(8,128)(2,1)S(1)}, u32[]{:S(2)}, u32[]{:S(2)}) %collective-permute-start.20) | collective-permute-done | bytes 786464 | tf_op jit(solution)/shard_map/ppermute | solution.py:22
  179.5 4.4 %collective-permute-start.21 = (bf16[192,2048]{1,0:T(8,128)(2,1)S(1)}, bf16[192,2048]{1,0:T(8,128)(2,1)S(1)}, u32[]{:S(2)}, u32[]{:S(2)}) collective-permute-start(bf16[192,2048]{1,0:T(8,128)(2,1)S(1)} %get-tuple-element.32), channel_id=1, source_target_pairs={{0,8},{4,12},{8,16},{12,20},{16,24},{20,28},{1,9},{5,13},{9,17},{1... | collective-permute-start | bytes 2359304 | tf_op jit(solution)/shard_map/ppermute | solution.py:22
  185.2 2.3 %multiply_convert_fusion.3 = bf16[192,1024]{1,0:T(8,128)(2,1)S(1)} fusion(f32[192,1024]{1,0:T(8,128)S(1)} %fusion.57, f32[192]{0:T(256)S(1)} %get-tuple-element.18, f32[192]{0:T(256)S(1)} %get-tuple-element.17, pred[1024]{0:T(1024)(128)(4,1)S(1)} %iota_compare_fusion.4, bf16[192,2048]{1,0:T(8,128)(2,1)S(1)} %copy-done.2, ...), kind=kOutput, calls=%fused_computation.43 | convolution fusion | flops 819462144 | bytes 6162944 | tf_op jit(solution)/shard_map/dot_general | solution.py:146
  189.8 8.2 %collective-permute-done.21 = bf16[192,2048]{1,0:T(8,128)(2,1)S(1)} collective-permute-done((bf16[192,2048]{1,0:T(8,128)(2,1)S(1)}, bf16[192,2048]{1,0:T(8,128)(2,1)S(1)}, u32[]{:S(2)}, u32[]{:S(2)}) %collective-permute-start.21) | collective-permute-done | bytes 786464 | tf_op jit(solution)/shard_map/ppermute | solution.py:22
  198.0 4.5 %collective-permute-done.18 = bf16[192,2048]{1,0:T(8,128)(2,1)S(1)} collective-permute-done((bf16[192,2048]{1,0:T(8,128)(2,1)S(1)}, bf16[192,2048]{1,0:T(8,128)(2,1)S(1)}, u32[]{:S(2)}, u32[]{:S(2)}) %collective-permute-start.18) | collective-permute-done | bytes 786464 | tf_op jit(solution)/shard_map/ppermute | solution.py:22
  (104 shorter events, 44.6 us)
Async XLA Ops:
  0.9 14.5 %collective-permute-start = (f32[2,512]{1,0:T(2,128)S(1)}, f32[2,512]{1,0:T(2,128)S(1)}, u32[]{:S(2)}, u32[]{:S(2)}) collective-permute-start(f32[2,512]{1,0:T(2,128)S(1)} %convert_multiply_fusion.3), channel_id=1, source_target_pairs={{0,4},{4,8},{8,12},{12,16},{16,20},{20,24},{24,28},{1,5},{5,9},{9,... | collective-permute-start | bytes 12296 | tf_op jit(solution)/shard_map/ppermute | solution.py:22
  8.3 26.3 %collective-permute-start.4 = (bf16[2048,256]{1,0:T(8,128)(2,1)}, bf16[2048,256]{1,0:T(8,128)(2,1)}, u32[]{:S(2)}, u32[]{:S(2)}) collective-permute-start(bf16[2048,256]{1,0:T(8,128)(2,1)} %dynamic-slice_bitcast_fusion.2), channel_id=1, source_target_pairs={{0,4},{4,0},{8,12},{12,8},{16,20},{20,16},{24,28},{28,24},{1,5},{5... | collective-permute-start | bytes 3145736 | tf_op jit(solution)/shard_map/ppermute | solution.py:26
  10.9 46.2 %collective-permute-start.6 = (bf16[2048,256]{1,0:T(8,128)(2,1)}, bf16[2048,256]{1,0:T(8,128)(2,1)}, u32[]{:S(2)}, u32[]{:S(2)}) collective-permute-start(bf16[2048,256]{1,0:T(8,128)(2,1)} %dynamic-slice_bitcast_fusion.1), channel_id=1, source_target_pairs={{0,4},{4,0},{8,12},{12,8},{16,20},{20,16},{24,28},{28,24},{1,5},{5... | collective-permute-start | bytes 3145736 | tf_op jit(solution)/shard_map/ppermute | solution.py:26
  12.4 65.7 %collective-permute-start.8 = (bf16[256,2048]{1,0:T(8,128)(2,1)}, bf16[256,2048]{1,0:T(8,128)(2,1)}, u32[]{:S(2)}, u32[]{:S(2)}) collective-permute-start(bf16[256,2048]{1,0:T(8,128)(2,1)} %dynamic-slice_bitcast_fusion), channel_id=1, source_target_pairs={{0,4},{4,0},{8,12},{12,8},{16,20},{20,16},{24,28},{28,24},{1,5},{5... | collective-permute-start | bytes 3145736 | tf_op jit(solution)/shard_map/ppermute | solution.py:26
  20.5 2.6 %collective-permute-start.2 = (bf16[192,2048]{1,0:T(8,128)(2,1)}, bf16[192,2048]{1,0:T(8,128)(2,1)}, u32[]{:S(2)}, u32[]{:S(2)}) collective-permute-start(bf16[192,2048]{1,0:T(8,128)(2,1)} %convolution_convert_fusion), channel_id=1, source_target_pairs={{0,1},{1,0},{2,3},{3,2},{4,5},{5,4},{6,7},{7,6},{8,9},{9,8},{10,11... | collective-permute-start | bytes 2359304 | tf_op jit(solution)/shard_map/ppermute | solution.py:26
  22.1 12.6 %collective-permute-start.1 = (bf16[192,2048]{1,0:T(8,128)(2,1)}, bf16[192,2048]{1,0:T(8,128)(2,1)}, u32[]{:S(2)}, u32[]{:S(2)}) collective-permute-start(bf16[192,2048]{1,0:T(8,128)(2,1)} %convolution_convert_fusion.1), channel_id=1, source_target_pairs={{0,1},{1,0},{2,3},{3,2},{4,5},{5,4},{6,7},{7,6},{8,9},{9,8},{10,11... | collective-permute-start | bytes 2359304 | tf_op jit(solution)/shard_map/ppermute | solution.py:26
  25.7 19.9 %collective-permute-start.3 = (bf16[192,2048]{1,0:T(8,128)(2,1)}, bf16[192,2048]{1,0:T(8,128)(2,1)}, u32[]{:S(2)}, u32[]{:S(2)}) collective-permute-start(bf16[192,2048]{1,0:T(8,128)(2,1)} %add_convert_fusion.5), channel_id=1, source_target_pairs={{0,2},{1,3},{2,0},{3,1},{4,6},{5,7},{6,4},{7,5},{8,10},{9,11},{10,... | collective-permute-start | bytes 2359304 | tf_op jit(solution)/shard_map/ppermute | solution.py:26
  28.1 19.6 %copy-start.5 = (bf16[192,2048]{1,0:T(8,128)(2,1)S(1)}, bf16[192,2048]{1,0:T(8,128)(2,1)}, u32[]{:S(2)}) copy-start(bf16[192,2048]{1,0:T(8,128)(2,1)} %param.21) | copy-start | bytes 2359300
  28.1 19.6 %copy-start.13 = (f32[2048]{0:T(1024)S(1)}, f32[2048]{0:T(1024)}, u32[]{:S(2)}) copy-start(f32[2048]{0:T(1024)} %param.22) | copy-start | bytes 24580
  34.6 43.5 %collective-permute-start.5 = (bf16[2048,256]{1,0:T(8,128)(2,1)}, bf16[2048,256]{1,0:T(8,128)(2,1)}, u32[]{:S(2)}, u32[]{:S(2)}) collective-permute-start(bf16[2048,256]{1,0:T(8,128)(2,1)} %collective-permute-done.4), channel_id=1, source_target_pairs={{0,1},{1,0},{2,3},{3,2},{4,5},{5,4},{6,7},{7,6},{8,9},{9,8},{10,11... | collective-permute-start | bytes 3145736 | tf_op jit(solution)/shard_map/ppermute | solution.py:26
  50.5 31.1 %collective-permute-start.11 = (bf16[192,2176]{1,0:T(8,128)(2,1)}, bf16[192,2176]{1,0:T(8,128)(2,1)}, u32[]{:S(2)}, u32[]{:S(2)}) collective-permute-start(bf16[192,2176]{1,0:T(8,128)(2,1)} %pad_maximum_fusion.4), channel_id=1, source_target_pairs={{0,8},{4,12},{8,16},{12,20},{16,24},{20,28},{1,9},{5,13},{9,17},{1... | collective-permute-start | bytes 2506760 | tf_op jit(solution)/shard_map/ppermute | solution.py:22
  55.0 27.5 %collective-permute-start.10 = (bf16[192,2176]{1,0:T(8,128)(2,1)}, bf16[192,2176]{1,0:T(8,128)(2,1)}, u32[]{:S(2)}, u32[]{:S(2)}) collective-permute-start(bf16[192,2176]{1,0:T(8,128)(2,1)} %pad_maximum_fusion.4), channel_id=1, source_target_pairs={{8,0},{12,4},{16,8},{20,12},{24,16},{28,20},{9,1},{13,5},{17,9},{2... | collective-permute-start | bytes 2506760 | tf_op jit(solution)/shard_map/ppermute | solution.py:22
  57.1 77.8 %collective-permute-start.7 = (bf16[2048,256]{1,0:T(8,128)(2,1)}, bf16[2048,256]{1,0:T(8,128)(2,1)S(1)}, u32[]{:S(2)}, u32[]{:S(2)}) collective-permute-start(bf16[2048,256]{1,0:T(8,128)(2,1)} %collective-permute-done.6), channel_id=1, source_target_pairs={{0,1},{1,0},{2,3},{3,2},{4,5},{5,4},{6,7},{7,6},{8,9},{9,8},{10,11... | collective-permute-start | bytes 3145736 | tf_op jit(solution)/shard_map/ppermute | solution.py:26
  78.2 59.2 %collective-permute-start.9 = (bf16[256,2048]{1,0:T(8,128)(2,1)}, bf16[256,2048]{1,0:T(8,128)(2,1)S(1)}, u32[]{:S(2)}, u32[]{:S(2)}) collective-permute-start(bf16[256,2048]{1,0:T(8,128)(2,1)} %collective-permute-done.8), channel_id=1, source_target_pairs={{0,1},{1,0},{2,3},{3,2},{4,5},{5,4},{6,7},{7,6},{8,9},{9,8},{10,11... | collective-permute-start | bytes 3145736 | tf_op jit(solution)/shard_map/ppermute | solution.py:26
  81.6 6.3 %collective-permute-start.13 = (bf16[192,2176]{1,0:T(8,128)(2,1)}, bf16[192,2176]{1,0:T(8,128)(2,1)S(1)}, u32[]{:S(2)}, u32[]{:S(2)}) collective-permute-start(bf16[192,2176]{1,0:T(8,128)(2,1)} %collective-permute-done.11), channel_id=1, source_target_pairs={{8,16},{12,20},{16,24},{20,28},{9,17},{13,21},{17,25},{21,29},{10,... | collective-permute-start | bytes 2506760 | tf_op jit(solution)/shard_map/ppermute | solution.py:22
  82.5 25.5 %collective-permute-start.12 = (bf16[192,2176]{1,0:T(8,128)(2,1)}, bf16[192,2176]{1,0:T(8,128)(2,1)S(1)}, u32[]{:S(2)}, u32[]{:S(2)}) collective-permute-start(bf16[192,2176]{1,0:T(8,128)(2,1)} %collective-permute-done.10), channel_id=1, source_target_pairs={{8,0},{12,4},{16,8},{20,12},{9,1},{13,5},{17,9},{21,13},{10,2},{14... | collective-permute-start | bytes 2506760 | tf_op jit(solution)/shard_map/ppermute | solution.py:22
  88.0 24.5 %collective-permute-start.14 = (bf16[192,2176]{1,0:T(8,128)(2,1)S(1)}, bf16[192,2176]{1,0:T(8,128)(2,1)S(1)}, u32[]{:S(2)}, u32[]{:S(2)}) collective-permute-start(bf16[192,2176]{1,0:T(8,128)(2,1)S(1)} %collective-permute-done.13), channel_id=1, source_target_pairs={{16,24},{20,28},{17,25},{21,29},{18,26},{22,30},{19,27},{23,31}} | collective-permute-start | bytes 2506760 | tf_op jit(solution)/shard_map/ppermute | solution.py:22
  108.0 22.0 %collective-permute-start.15 = (bf16[192,2176]{1,0:T(8,128)(2,1)S(1)}, bf16[192,2176]{1,0:T(8,128)(2,1)S(1)}, u32[]{:S(2)}, u32[]{:S(2)}) collective-permute-start(bf16[192,2176]{1,0:T(8,128)(2,1)S(1)} %collective-permute-done.12), channel_id=1, source_target_pairs={{8,0},{12,4},{9,1},{13,5},{10,2},{14,6},{11,3},{15,7}} | collective-permute-start | bytes 2506760 | tf_op jit(solution)/shard_map/ppermute | solution.py:22
  139.7 6.8 %collective-permute-start.16 = (bf16[192,2048]{1,0:T(8,128)(2,1)S(1)}, bf16[192,2048]{1,0:T(8,128)(2,1)S(1)}, u32[]{:S(2)}, u32[]{:S(2)}) collective-permute-start(bf16[192,2048]{1,0:T(8,128)(2,1)S(1)} %convert_element_type.142), channel_id=1, source_target_pairs={{24,16},{28,20},{25,17},{29,21},{26,18},{30,22},{27,19},{31,23}} | collective-permute-start | bytes 2359304 | tf_op jit(solution)/shard_map/ppermute | solution.py:22
  140.4 17.3 %collective-permute-start.19 = (bf16[192,2048]{1,0:T(8,128)(2,1)S(1)}, bf16[192,2048]{1,0:T(8,128)(2,1)S(1)}, u32[]{:S(2)}, u32[]{:S(2)}) collective-permute-start(bf16[192,2048]{1,0:T(8,128)(2,1)S(1)} %convert_element_type.142), channel_id=1, source_target_pairs={{0,8},{4,12},{1,9},{5,13},{2,10},{6,14},{3,11},{7,15}} | collective-permute-start | bytes 2359304 | tf_op jit(solution)/shard_map/ppermute | solution.py:22
  158.2 10.3 %collective-permute-start.17 = (bf16[192,2048]{1,0:T(8,128)(2,1)S(1)}, bf16[192,2048]{1,0:T(8,128)(2,1)S(1)}, u32[]{:S(2)}, u32[]{:S(2)}) collective-permute-start(bf16[192,2048]{1,0:T(8,128)(2,1)S(1)} %get-tuple-element.33), channel_id=1, source_target_pairs={{16,8},{20,12},{24,16},{28,20},{17,9},{21,13},{25,17},{29,21},{18,... | collective-permute-start | bytes 2359304 | tf_op jit(solution)/shard_map/ppermute | solution.py:22
  159.0 20.0 %collective-permute-start.20 = (bf16[192,2048]{1,0:T(8,128)(2,1)S(1)}, bf16[192,2048]{1,0:T(8,128)(2,1)S(1)}, u32[]{:S(2)}, u32[]{:S(2)}) collective-permute-start(bf16[192,2048]{1,0:T(8,128)(2,1)S(1)} %get-tuple-element.34), channel_id=1, source_target_pairs={{0,8},{4,12},{8,16},{12,20},{1,9},{5,13},{9,17},{13,21},{2,10},{6,... | collective-permute-start | bytes 2359304 | tf_op jit(solution)/shard_map/ppermute | solution.py:22
  179.5 18.5 %collective-permute-start.21 = (bf16[192,2048]{1,0:T(8,128)(2,1)S(1)}, bf16[192,2048]{1,0:T(8,128)(2,1)S(1)}, u32[]{:S(2)}, u32[]{:S(2)}) collective-permute-start(bf16[192,2048]{1,0:T(8,128)(2,1)S(1)} %get-tuple-element.32), channel_id=1, source_target_pairs={{0,8},{4,12},{8,16},{12,20},{16,24},{20,28},{1,9},{5,13},{9,17},{1... | collective-permute-start | bytes 2359304 | tf_op jit(solution)/shard_map/ppermute | solution.py:22
  183.9 18.6 %collective-permute-start.18 = (bf16[192,2048]{1,0:T(8,128)(2,1)S(1)}, bf16[192,2048]{1,0:T(8,128)(2,1)S(1)}, u32[]{:S(2)}, u32[]{:S(2)}) collective-permute-start(bf16[192,2048]{1,0:T(8,128)(2,1)S(1)} %get-tuple-element.31), channel_id=1, source_target_pairs={{8,0},{12,4},{16,8},{20,12},{24,16},{28,20},{9,1},{13,5},{17,9},{2... | collective-permute-start | bytes 2359304 | tf_op jit(solution)/shard_map/ppermute | solution.py:22
  (16 other events, 98.1 us)
where the time goes:
time: 205 us; the launch traced here: 204 us
  waiting for transfers between devices  111 us (54%)
  matrix products  36.7 us (18%)
  starting transfers between devices  34.1 us (17%)
  other arithmetic  15.7 us (8%)
  local copies, waits for them, and re-layouts  5.69 us (3%)
    ppermute x13, waiting for transfers between devices, shifted(): return lax.ppermute(value, 'sp', [(s, s + steps) for s in senders])  71.2 us
    ppermute x9, waiting for transfers between devices, swapped(): lax.ppermute(value, axis, [(s, s ^ bit) for s in range(lax.axis_size(axis...  39.9 us
    ppermute x13, starting transfers between devices, shifted(): return lax.ppermute(value, 'sp', [(s, s + steps) for s in senders])  28.6 us
    dot_general x4, matrix products, served(): first = jnp.dot(rows, gate_both, preferred_element_type=jnp.float32)  12.3 us
    dot_general x4, matrix products, served(): second = jnp.dot(rows, up_both, preferred_element_type=jnp.float32)  9.24 us
    dot_general x4, matrix products, served(): jnp.dot(hidden, down_both, preferred_element_type=jnp.float32)  9.03 us
    convert_element_type x7, other arithmetic, bf16(): return value.astype(jnp.bfloat16)  6.61 us
    dot_general x4, matrix products, partial(): return jnp.dot(rows, out_weight, preferred_element_type=jnp.float32)  6.15 us
  transfers between devices with their start and end apart: 22, of which 11 were waited for; matrix products, arithmetic and copies ran while one was open for 25% of the time, Pallas kernels for 0%

commit v1 on v0

--- a/solution.py
+++ b/solution.py
@@ -52,7 +52,8 @@
         if bit == 1:
             return partial(me ^ owner_bits)
         half = bit // 2
-        given = swapped(bf16(total(owner_bits | half, half)), "tp", half)
+        sent = bf16(total(owner_bits | half, half))
+        given = swapped(sent, "tp", half)
         return total(owner_bits, half) + f32(given)
 
     return total(0, parts)
@@ -135,17 +136,16 @@
     depth = normed.shape[1]
 
     def served(block):
-        rows, shares = block[:, :depth], f32(block[:, depth:])
-
-        def share_of(expert):
-            chosen = (column == expert) | (column == expert + count)
-            return jnp.sum(jnp.where(chosen, shares, 0.0), axis=1, keepdims=True)
-
+        rows = block[:, :depth]
+        chosen = jnp.arange(lanes, dtype=jnp.int32)[:, None] % count
+        picks = bf16(chosen == jnp.stack([me, me ^ 1])[None, :])
+        picks = jnp.where(jnp.arange(lanes)[:, None] < 2 * count, picks, 0)
+        shares = jnp.dot(block[:, depth:], picks, preferred_element_type=jnp.float32)
         wide = 2 * half
         first = jnp.dot(rows, gate_both, preferred_element_type=jnp.float32)
         second = jnp.dot(rows, up_both, preferred_element_type=jnp.float32)
         mine = jnp.arange(2 * wide)[None, :] < wide
-        share = jnp.where(mine, share_of(me), share_of(me ^ 1))
+        share = jnp.where(mine, shares[:, :1], shares[:, 1:])
         hidden = lax.optimization_barrier(bf16(jax.nn.silu(first) * second * share))
         return lax.optimization_barrier(
             jnp.dot(hidden, down_both, preferred_element_type=jnp.float32)

time: 205 us -> 221 us (1.078)
  waiting for transfers between devices: 111 us -> 125 us
    ppermute x9, waiting for transfers between devices: 39.9 us -> 49.4 us  [swapped(): lax.ppermute(value, axis, [(s, s ^ bit) for s in range(lax.axis_size(axis...]
    ppermute x13, waiting for transfers between devices: 71.2 us -> 75.3 us  [shifted(): return lax.ppermute(value, 'sp', [(s, s + steps) for s in senders])]
  transfers between devices with their start and end apart: 22 -> 22, of which waited for: 11 -> 10; matrix products, arithmetic and copies ran while one was open for 25% -> 24% of each run, Pallas kernels for 0% -> 0%
where the time goes in v1:
time: 221 us; the launch traced here: 220 us
  waiting for transfers between devices  125 us (57%)
  matrix products  37.8 us (17%)
  starting transfers between devices  35.2 us (16%)
  other arithmetic  15.1 us (7%)
  local copies, waits for them, and re-layouts  7.02 us (3%)
    ppermute x13, waiting for transfers between devices, shifted(): return lax.ppermute(value, 'sp', [(s, s + steps) for s in senders])  75.3 us
    ppermute x9, waiting for transfers between devices, swapped(): lax.ppermute(value, axis, [(s, s ^ bit) for s in range(lax.axis_size(axis...  49.4 us
    ppermute x13, starting transfers between devices, shifted(): return lax.ppermute(value, 'sp', [(s, s + steps) for s in senders])  29.1 us
    dot_general x4, matrix products, served(): first = jnp.dot(rows, gate_both, preferred_element_type=jnp.float32)  12.2 us
    dot_general x4, matrix products, served(): second = jnp.dot(rows, up_both, preferred_element_type=jnp.float32)  9.31 us
    dot_general x4, matrix products, served(): jnp.dot(hidden, down_both, preferred_element_type=jnp.float32)  9.11 us
    convert_element_type x7, other arithmetic, bf16(): return value.astype(jnp.bfloat16)  6.49 us
    ppermute x9, starting transfers between devices, swapped(): lax.ppermute(value, axis, [(s, s ^ bit) for s in range(lax.axis_size(axis...  6.12 us
  transfers between devices with their start and end apart: 22, of which 10 were waited for; matrix products, arithmetic and copies ran while one was open for 24% of the time, Pallas kernels for 0%

profile of v1, /device:TPU:0, one launch (start us, length us, event | category | flops | bytes accessed | tf_op | source)
XLA Modules:
  0.0 220.3 jit_solution(8591663416153718047)
XLA Ops:
  0.9 4.9 %collective-permute-start = (f32[2,512]{1,0:T(2,128)S(1)}, f32[2,512]{1,0:T(2,128)S(1)}, u32[]{:S(2)}, u32[]{:S(2)}) collective-permute-start(f32[2,512]{1,0:T(2,128)S(1)} %convert_multiply_fusion.3), channel_id=1, source_target_pairs={{0,4},{4,8},{8,12},{12,16},{16,20},{20,24},{24,28},{1,5},{5,9},{9,... | collective-permute-start | bytes 12296 | tf_op jit(solution)/shard_map/ppermute | solution.py:22
  5.8 2.5 %dynamic-slice_bitcast_fusion = bf16[256,2048]{1,0:T(8,128)(2,1)} fusion(bf16[1,512,2048]{2,1,0:T(8,128)(2,1)} %param.29, s32[]{:T(128)S(6)} %select_n.116), kind=kLoop, calls=%fused_computation.33 | loop fusion | bytes 2097156 | tf_op jit(solution)/shard_map/dynamic_slice | solution.py:88
  9.8 2.3 %dynamic-slice_bitcast_fusion.1 = bf16[2048,256]{1,0:T(8,128)(2,1)} fusion(bf16[1,2048,512]{2,1,0:T(8,128)(2,1)} %param.28, s32[]{:T(128)S(6)} %select_n.116), kind=kLoop, calls=%fused_computation.34 | loop fusion | bytes 2097156 | tf_op jit(solution)/shard_map/dynamic_slice | solution.py:88
  16.8 3.5 %fusion.5 = bf16[768,512]{1,0:T(8,128)(2,1)S(1)} fusion(f32[2,512]{1,0:T(2,128)S(1)} %collective-permute-done, f32[768,512]{1,0:T(8,128)} %convert_multiply_fusion.2, bf16[768,512]{1,0:T(8,128)(2,1)} %param.15, f32[512]{0:T(512)S(1)} %bitcast.73, f32[512]{0:T(512)S(1)} %bitcast.74, f32[512]{0:T(512)S(1)} %bitcast.72), kind=kLoop, calls=%fused_computation.15 | loop fusion | flops 3932160 | bytes 3155968 | tf_op jit(solution)/shard_map/convert_element_type | solution.py:14
  24.3 2.6 %add_convert_fusion.5 = bf16[192,2048]{1,0:T(8,128)(2,1)} fusion(bf16[192,2048]{1,0:T(8,128)(2,1)} %collective-permute-done.2, bf16[512,2048]{1,0:T(8,128)(2,1)S(1)} %copy-done, bf16[4,192,512]{2,1,0:T(8,128)(2,1)S(1)} %bitcast.58, s32[]{:T(128)S(6)} %select_n.113), kind=kOutput, calls=%fused_computation.31 | convolution fusion | flops 403832832 | bytes 3866628 | tf_op jit(solution)/shard_map/dot_general | solution.py:49
  29.4 48.8 %collective-permute-done.4 = bf16[2048,256]{1,0:T(8,128)(2,1)} collective-permute-done((bf16[2048,256]{1,0:T(8,128)(2,1)}, bf16[2048,256]{1,0:T(8,128)(2,1)}, u32[]{:S(2)}, u32[]{:S(2)}) %collective-permute-start.4) | collective-permute-done | bytes 1048608 | tf_op jit(solution)/shard_map/ppermute | solution.py:26
  83.1 4.5 %collective-permute-start.11 = (bf16[192,2176]{1,0:T(8,128)(2,1)}, bf16[192,2176]{1,0:T(8,128)(2,1)}, u32[]{:S(2)}, u32[]{:S(2)}) collective-permute-start(bf16[192,2176]{1,0:T(8,128)(2,1)} %pad_maximum_fusion.4), channel_id=1, source_target_pairs={{0,8},{4,12},{8,16},{12,20},{16,24},{20,28},{1,9},{5,13},{9,17},{1... | collective-permute-start | bytes 2506760 | tf_op jit(solution)/shard_map/ppermute | solution.py:22
  89.7 3.4 %fusion.81 = f32[192,1024]{1,0:T(8,128)S(1)} fusion(bf16[192,2048]{1,0:T(8,128)(2,1)} %copy-done.1, bf16[2048,256]{1,0:T(8,128)(2,1)} %collective-permute-done.5, bf16[2048,256]{1,0:T(8,128)(2,1)} %collective-permute-done.4, bf16[2048,512]{1,0:T(8,128)(2,1)} %bitcast.60), kind=kOutput, calls=%fused_computation.118 | convolution fusion | flops 817889280 | bytes 5767168 | tf_op jit(solution)/shard_map/dot_general | solution.py:145
  93.2 12.2 %collective-permute-done.11 = bf16[192,2176]{1,0:T(8,128)(2,1)} collective-permute-done((bf16[192,2176]{1,0:T(8,128)(2,1)}, bf16[192,2176]{1,0:T(8,128)(2,1)}, u32[]{:S(2)}, u32[]{:S(2)}) %collective-permute-start.11) | collective-permute-done | bytes 835616 | tf_op jit(solution)/shard_map/ppermute | solution.py:22
  106.1 4.4 %collective-permute-done.10 = bf16[192,2176]{1,0:T(8,128)(2,1)} collective-permute-done((bf16[192,2176]{1,0:T(8,128)(2,1)}, bf16[192,2176]{1,0:T(8,128)(2,1)}, u32[]{:S(2)}, u32[]{:S(2)}) %collective-permute-start.10) | collective-permute-done | bytes 835616 | tf_op jit(solution)/shard_map/ppermute | solution.py:22
  113.3 2.9 %fusion.27 = f32[192,1024]{1,0:T(8,128)S(1)} fusion(bf16[192,2176]{1,0:T(8,128)(2,1)S(1)} %broadcast_select_fusion.1, bf16[2048,256]{1,0:T(8,128)(2,1)} %collective-permute-done.5, bf16[2048,256]{1,0:T(8,128)(2,1)} %collective-permute-done.4, bf16[2048,512]{1,0:T(8,128)(2,1)S(1)} %bitcast.61), kind=kOutput, calls=%fused_computation.54 | convolution fusion | flops 817889280 | bytes 5767168 | tf_op jit(solution)/shard_map/dot_general | solution.py:145
  116.9 15.5 %collective-permute-done.12 = bf16[192,2176]{1,0:T(8,128)(2,1)S(1)} collective-permute-done((bf16[192,2176]{1,0:T(8,128)(2,1)}, bf16[192,2176]{1,0:T(8,128)(2,1)S(1)}, u32[]{:S(2)}, u32[]{:S(2)}) %collective-permute-start.12) | collective-permute-done | bytes 835616 | tf_op jit(solution)/shard_map/ppermute | solution.py:22
  134.3 2.9 %fusion.21 = f32[192,1024]{1,0:T(8,128)S(1)} fusion(bf16[192,2176]{1,0:T(8,128)(2,1)S(1)} %broadcast_select_fusion, bf16[2048,256]{1,0:T(8,128)(2,1)} %collective-permute-done.5, bf16[2048,256]{1,0:T(8,128)(2,1)} %collective-permute-done.4, bf16[2048,512]{1,0:T(8,128)(2,1)S(1)} %bitcast.62), kind=kOutput, calls=%fused_computation.50 | convolution fusion | flops 817889280 | bytes 5767168 | tf_op jit(solution)/shard_map/dot_general | solution.py:145
  137.1 16.2 %collective-permute-done.15 = bf16[192,2176]{1,0:T(8,128)(2,1)S(1)} collective-permute-done((bf16[192,2176]{1,0:T(8,128)(2,1)S(1)}, bf16[192,2176]{1,0:T(8,128)(2,1)S(1)}, u32[]{:S(2)}, u32[]{:S(2)}) %collective-permute-start.15) | collective-permute-done | bytes 835616 | tf_op jit(solution)/shard_map/ppermute | solution.py:22
  154.9 3.0 %fusion.15 = f32[192,1024]{1,0:T(8,128)S(1)} fusion(bf16[192,2176]{1,0:T(8,128)(2,1)S(1)} %select_select_fusion, bf16[2048,256]{1,0:T(8,128)(2,1)} %collective-permute-done.5, bf16[2048,256]{1,0:T(8,128)(2,1)} %collective-permute-done.4, bf16[2048,512]{1,0:T(8,128)(2,1)S(1)} %bitcast.63), kind=kOutput, calls=%fused_computation.46 | convolution fusion | flops 817889280 | bytes 5767168 | tf_op jit(solution)/shard_map/dot_general | solution.py:145
  157.9 2.4 %multiply_convert_fusion = bf16[192,1024]{1,0:T(8,128)(2,1)S(1)} fusion(f32[192,1024]{1,0:T(8,128)S(1)} %fusion.15, bf16[192,2176]{1,0:T(8,128)(2,1)S(1)} %select_select_fusion, f32[192]{0:T(256)S(1)} %bitcast.90, f32[192]{0:T(256)S(1)} %bitcast.89, pred[1024]{0:T(1024)(128)(4,1)S(1)} %iota_compare_fusion.4, ...), kind=kOutput, calls=%fused_computation.40 | convolution fusion | flops 819462144 | bytes 6163456 | tf_op jit(solution)/shard_map/dot_general | solution.py:146
  165.0 2.3 %multiply_convert_fusion.1 = bf16[192,1024]{1,0:T(8,128)(2,1)S(1)} fusion(f32[192,1024]{1,0:T(8,128)S(1)} %fusion.21, bf16[192,2176]{1,0:T(8,128)(2,1)S(1)} %broadcast_select_fusion, f32[192]{0:T(256)S(1)} %bitcast.88, f32[192]{0:T(256)S(1)} %bitcast.87, pred[1024]{0:T(1024)(128)(4,1)S(1)} %iota_compare_fusion.4, ...), kind=kOutput, calls=%fused_computation.41 | convolution fusion | flops 819462144 | bytes 6163456 | tf_op jit(solution)/shard_map/dot_general | solution.py:146
  169.6 9.4 %collective-permute-done.19 = bf16[192,2048]{1,0:T(8,128)(2,1)S(1)} collective-permute-done((bf16[192,2048]{1,0:T(8,128)(2,1)S(1)}, bf16[192,2048]{1,0:T(8,128)(2,1)S(1)}, u32[]{:S(2)}, u32[]{:S(2)}) %collective-permute-start.19) | collective-permute-done | bytes 786464 | tf_op jit(solution)/shard_map/ppermute | solution.py:22
  180.2 5.0 %collective-permute-start.20 = (bf16[192,2048]{1,0:T(8,128)(2,1)S(1)}, bf16[192,2048]{1,0:T(8,128)(2,1)S(1)}, u32[]{:S(2)}, u32[]{:S(2)}) collective-permute-start(bf16[192,2048]{1,0:T(8,128)(2,1)S(1)} %get-tuple-element.20), channel_id=1, source_target_pairs={{0,8},{4,12},{8,16},{12,20},{1,9},{5,13},{9,17},{13,21},{2,10},{6,... | collective-permute-start | bytes 2359304 | tf_op jit(solution)/shard_map/ppermute | solution.py:22
  185.2 2.3 %multiply_convert_fusion.2 = bf16[192,1024]{1,0:T(8,128)(2,1)S(1)} fusion(f32[192,1024]{1,0:T(8,128)S(1)} %fusion.27, bf16[192,2176]{1,0:T(8,128)(2,1)S(1)} %broadcast_select_fusion.1, f32[192]{0:T(256)S(1)} %bitcast.86, f32[192]{0:T(256)S(1)} %bitcast.85, pred[1024]{0:T(1024)(128)(4,1)S(1)} %iota_compare_fusion.4, ...), kind=kOutput, calls=%fused_computation.42 | convolution fusion | flops 819462144 | bytes 6163456 | tf_op jit(solution)/shard_map/dot_general | solution.py:146
  189.8 9.2 %collective-permute-done.20 = bf16[192,2048]{1,0:T(8,128)(2,1)S(1)} collective-permute-done((bf16[192,2048]{1,0:T(8,128)(2,1)S(1)}, bf16[192,2048]{1,0:T(8,128)(2,1)S(1)}, u32[]{:S(2)}, u32[]{:S(2)}) %collective-permute-start.20) | collective-permute-done | bytes 786464 | tf_op jit(solution)/shard_map/ppermute | solution.py:22
  200.9 5.1 %collective-permute-start.21 = (bf16[192,2048]{1,0:T(8,128)(2,1)S(1)}, bf16[192,2048]{1,0:T(8,128)(2,1)S(1)}, u32[]{:S(2)}, u32[]{:S(2)}) collective-permute-start(bf16[192,2048]{1,0:T(8,128)(2,1)S(1)} %get-tuple-element.18), channel_id=1, source_target_pairs={{0,8},{4,12},{8,16},{12,20},{16,24},{20,28},{1,9},{5,13},{9,17},{1... | collective-permute-start | bytes 2359304 | tf_op jit(solution)/shard_map/ppermute | solution.py:22
  205.9 2.3 %multiply_convert_fusion.3 = bf16[192,1024]{1,0:T(8,128)(2,1)S(1)} fusion(f32[192,1024]{1,0:T(8,128)S(1)} %fusion.81, f32[192]{0:T(256)S(1)} %bitcast.84, f32[192]{0:T(256)S(1)} %bitcast.83, pred[1024]{0:T(1024)(128)(4,1)S(1)} %iota_compare_fusion.4, bf16[192,2048]{1,0:T(8,128)(2,1)S(1)} %copy-done.2, bf16[2048,256]{1,0:T(8,128)(2,1)S(1)} %collective-permute-done.7, ...), kind=kOutput, calls=%fused_computation.43 | convolution fusion | flops 819462144 | bytes 6162944 | tf_op jit(solution)/shard_map/dot_general | solution.py:146
  210.5 7.2 %collective-permute-done.18 = bf16[192,2048]{1,0:T(8,128)(2,1)S(1)} collective-permute-done((bf16[192,2048]{1,0:T(8,128)(2,1)S(1)}, bf16[192,2048]{1,0:T(8,128)(2,1)S(1)}, u32[]{:S(2)}, u32[]{:S(2)}) %collective-permute-start.18) | collective-permute-done | bytes 786464 | tf_op jit(solution)/shard_map/ppermute | solution.py:22
  (110 shorter events, 45.1 us)
Async XLA Ops:
  0.9 15.9 %collective-permute-start = (f32[2,512]{1,0:T(2,128)S(1)}, f32[2,512]{1,0:T(2,128)S(1)}, u32[]{:S(2)}, u32[]{:S(2)}) collective-permute-start(f32[2,512]{1,0:T(2,128)S(1)} %convert_multiply_fusion.3), channel_id=1, source_target_pairs={{0,4},{4,8},{8,12},{12,16},{16,20},{20,24},{24,28},{1,5},{5,9},{9,... | collective-permute-start | bytes 12296 | tf_op jit(solution)/shard_map/ppermute | solution.py:22
  8.3 80.8 %collective-permute-start.8 = (bf16[256,2048]{1,0:T(8,128)(2,1)}, bf16[256,2048]{1,0:T(8,128)(2,1)}, u32[]{:S(2)}, u32[]{:S(2)}) collective-permute-start(bf16[256,2048]{1,0:T(8,128)(2,1)} %dynamic-slice_bitcast_fusion), channel_id=1, source_target_pairs={{0,4},{4,0},{8,12},{12,8},{16,20},{20,16},{24,28},{28,24},{1,5},{5... | collective-permute-start | bytes 3145736 | tf_op jit(solution)/shard_map/ppermute | solution.py:26
  12.1 77.3 %collective-permute-start.6 = (bf16[2048,256]{1,0:T(8,128)(2,1)}, bf16[2048,256]{1,0:T(8,128)(2,1)}, u32[]{:S(2)}, u32[]{:S(2)}) collective-permute-start(bf16[2048,256]{1,0:T(8,128)(2,1)} %dynamic-slice_bitcast_fusion.1), channel_id=1, source_target_pairs={{0,4},{4,0},{8,12},{12,8},{16,20},{20,16},{24,28},{28,24},{1,5},{5... | collective-permute-start | bytes 3145736 | tf_op jit(solution)/shard_map/ppermute | solution.py:26
  13.7 64.5 %collective-permute-start.4 = (bf16[2048,256]{1,0:T(8,128)(2,1)}, bf16[2048,256]{1,0:T(8,128)(2,1)}, u32[]{:S(2)}, u32[]{:S(2)}) collective-permute-start(bf16[2048,256]{1,0:T(8,128)(2,1)} %dynamic-slice_bitcast_fusion.2), channel_id=1, source_target_pairs={{0,4},{4,0},{8,12},{12,8},{16,20},{20,16},{24,28},{28,24},{1,5},{5... | collective-permute-start | bytes 3145736 | tf_op jit(solution)/shard_map/ppermute | solution.py:26
  21.7 2.6 %collective-permute-start.2 = (bf16[192,2048]{1,0:T(8,128)(2,1)}, bf16[192,2048]{1,0:T(8,128)(2,1)}, u32[]{:S(2)}, u32[]{:S(2)}) collective-permute-start(bf16[192,2048]{1,0:T(8,128)(2,1)} %convolution_convert_fusion), channel_id=1, source_target_pairs={{0,1},{1,0},{2,3},{3,2},{4,5},{5,4},{6,7},{7,6},{8,9},{9,8},{10,11... | collective-permute-start | bytes 2359304 | tf_op jit(solution)/shard_map/ppermute | solution.py:26
  23.2 55.0 %collective-permute-start.1 = (bf16[192,2048]{1,0:T(8,128)(2,1)}, bf16[192,2048]{1,0:T(8,128)(2,1)}, u32[]{:S(2)}, u32[]{:S(2)}) collective-permute-start(bf16[192,2048]{1,0:T(8,128)(2,1)} %convolution_convert_fusion.1), channel_id=1, source_target_pairs={{0,1},{1,0},{2,3},{3,2},{4,5},{5,4},{6,7},{7,6},{8,9},{9,8},{10,11... | collective-permute-start | bytes 2359304 | tf_op jit(solution)/shard_map/ppermute | solution.py:26
  26.9 51.2 %collective-permute-start.3 = (bf16[192,2048]{1,0:T(8,128)(2,1)}, bf16[192,2048]{1,0:T(8,128)(2,1)}, u32[]{:S(2)}, u32[]{:S(2)}) collective-permute-start(bf16[192,2048]{1,0:T(8,128)(2,1)} %add_convert_fusion.5), channel_id=1, source_target_pairs={{0,2},{1,3},{2,0},{3,1},{4,6},{5,7},{6,4},{7,5},{8,10},{9,11},{10,... | collective-permute-start | bytes 2359304 | tf_op jit(solution)/shard_map/ppermute | solution.py:26
  29.4 50.9 %copy-start.5 = (bf16[192,2048]{1,0:T(8,128)(2,1)S(1)}, bf16[192,2048]{1,0:T(8,128)(2,1)}, u32[]{:S(2)}) copy-start(bf16[192,2048]{1,0:T(8,128)(2,1)} %param.21) | copy-start | bytes 2359300
  29.4 50.9 %copy-start.12 = (f32[2048]{0:T(1024)S(1)}, f32[2048]{0:T(1024)}, u32[]{:S(2)}) copy-start(f32[2048]{0:T(1024)} %param.22) | copy-start | bytes 24580
  78.2 11.5 %collective-permute-start.5 = (bf16[2048,256]{1,0:T(8,128)(2,1)}, bf16[2048,256]{1,0:T(8,128)(2,1)}, u32[]{:S(2)}, u32[]{:S(2)}) collective-permute-start(bf16[2048,256]{1,0:T(8,128)(2,1)} %collective-permute-done.4), channel_id=1, source_target_pairs={{0,1},{1,0},{2,3},{3,2},{4,5},{5,4},{6,7},{7,6},{8,9},{9,8},{10,11... | collective-permute-start | bytes 3145736 | tf_op jit(solution)/shard_map/ppermute | solution.py:26
  83.1 22.3 %collective-permute-start.11 = (bf16[192,2176]{1,0:T(8,128)(2,1)}, bf16[192,2176]{1,0:T(8,128)(2,1)}, u32[]{:S(2)}, u32[]{:S(2)}) collective-permute-start(bf16[192,2176]{1,0:T(8,128)(2,1)} %pad_maximum_fusion.4), channel_id=1, source_target_pairs={{0,8},{4,12},{8,16},{12,20},{16,24},{20,28},{1,9},{5,13},{9,17},{1... | collective-permute-start | bytes 2506760 | tf_op jit(solution)/shard_map/ppermute | solution.py:22
  87.5 22.9 %collective-permute-start.10 = (bf16[192,2176]{1,0:T(8,128)(2,1)}, bf16[192,2176]{1,0:T(8,128)(2,1)}, u32[]{:S(2)}, u32[]{:S(2)}) collective-permute-start(bf16[192,2176]{1,0:T(8,128)(2,1)} %pad_maximum_fusion.4), channel_id=1, source_target_pairs={{8,0},{12,4},{16,8},{20,12},{24,16},{28,20},{9,1},{13,5},{17,9},{2... | collective-permute-start | bytes 2506760 | tf_op jit(solution)/shard_map/ppermute | solution.py:22
  89.1 71.3 %collective-permute-start.9 = (bf16[256,2048]{1,0:T(8,128)(2,1)}, bf16[256,2048]{1,0:T(8,128)(2,1)S(1)}, u32[]{:S(2)}, u32[]{:S(2)}) collective-permute-start(bf16[256,2048]{1,0:T(8,128)(2,1)} %collective-permute-done.8), channel_id=1, source_target_pairs={{0,1},{1,0},{2,3},{3,2},{4,5},{5,4},{6,7},{7,6},{8,9},{9,8},{10,11... | collective-permute-start | bytes 3145736 | tf_op jit(solution)/shard_map/ppermute | solution.py:26
  89.4 68.5 %collective-permute-start.7 = (bf16[2048,256]{1,0:T(8,128)(2,1)}, bf16[2048,256]{1,0:T(8,128)(2,1)S(1)}, u32[]{:S(2)}, u32[]{:S(2)}) collective-permute-start(bf16[2048,256]{1,0:T(8,128)(2,1)} %collective-permute-done.6), channel_id=1, source_target_pairs={{0,1},{1,0},{2,3},{3,2},{4,5},{5,4},{6,7},{7,6},{8,9},{9,8},{10,11... | collective-permute-start | bytes 3145736 | tf_op jit(solution)/shard_map/ppermute | solution.py:26
  105.4 10.8 %collective-permute-start.13 = (bf16[192,2176]{1,0:T(8,128)(2,1)}, bf16[192,2176]{1,0:T(8,128)(2,1)S(1)}, u32[]{:S(2)}, u32[]{:S(2)}) collective-permute-start(bf16[192,2176]{1,0:T(8,128)(2,1)} %collective-permute-done.11), channel_id=1, source_target_pairs={{8,16},{12,20},{16,24},{20,28},{9,17},{13,21},{17,25},{21,29},{10,... | collective-permute-start | bytes 2506760 | tf_op jit(solution)/shard_map/ppermute | solution.py:22
  110.5 22.0 %collective-permute-start.12 = (bf16[192,2176]{1,0:T(8,128)(2,1)}, bf16[192,2176]{1,0:T(8,128)(2,1)S(1)}, u32[]{:S(2)}, u32[]{:S(2)}) collective-permute-start(bf16[192,2176]{1,0:T(8,128)(2,1)} %collective-permute-done.10), channel_id=1, source_target_pairs={{8,0},{12,4},{16,8},{20,12},{9,1},{13,5},{17,9},{21,13},{10,2},{14... | collective-permute-start | bytes 2506760 | tf_op jit(solution)/shard_map/ppermute | solution.py:22
  116.2 20.9 %collective-permute-start.14 = (bf16[192,2176]{1,0:T(8,128)(2,1)S(1)}, bf16[192,2176]{1,0:T(8,128)(2,1)S(1)}, u32[]{:S(2)}, u32[]{:S(2)}) collective-permute-start(bf16[192,2176]{1,0:T(8,128)(2,1)S(1)} %collective-permute-done.13), channel_id=1, source_target_pairs={{16,24},{20,28},{17,25},{21,29},{18,26},{22,30},{19,27},{23,31}} | collective-permute-start | bytes 2506760 | tf_op jit(solution)/shard_map/ppermute | solution.py:22
  132.4 20.9 %collective-permute-start.15 = (bf16[192,2176]{1,0:T(8,128)(2,1)S(1)}, bf16[192,2176]{1,0:T(8,128)(2,1)S(1)}, u32[]{:S(2)}, u32[]{:S(2)}) collective-permute-start(bf16[192,2176]{1,0:T(8,128)(2,1)S(1)} %collective-permute-done.12), channel_id=1, source_target_pairs={{8,0},{12,4},{9,1},{13,5},{10,2},{14,6},{11,3},{15,7}} | collective-permute-start | bytes 2506760 | tf_op jit(solution)/shard_map/ppermute | solution.py:22
  162.8 16.2 %collective-permute-start.19 = (bf16[192,2048]{1,0:T(8,128)(2,1)S(1)}, bf16[192,2048]{1,0:T(8,128)(2,1)S(1)}, u32[]{:S(2)}, u32[]{:S(2)}) collective-permute-start(bf16[192,2048]{1,0:T(8,128)(2,1)S(1)} %convert_element_type.138), channel_id=1, source_target_pairs={{0,8},{4,12},{1,9},{5,13},{2,10},{6,14},{3,11},{7,15}} | collective-permute-start | bytes 2359304 | tf_op jit(solution)/shard_map/ppermute | solution.py:22
  164.3 14.7 %collective-permute-start.16 = (bf16[192,2048]{1,0:T(8,128)(2,1)S(1)}, bf16[192,2048]{1,0:T(8,128)(2,1)S(1)}, u32[]{:S(2)}, u32[]{:S(2)}) collective-permute-start(bf16[192,2048]{1,0:T(8,128)(2,1)S(1)} %convert_element_type.138), channel_id=1, source_target_pairs={{24,16},{28,20},{25,17},{29,21},{26,18},{30,22},{27,19},{31,23}} | collective-permute-start | bytes 2359304 | tf_op jit(solution)/shard_map/ppermute | solution.py:22
  179.4 10.3 %collective-permute-start.17 = (bf16[192,2048]{1,0:T(8,128)(2,1)S(1)}, bf16[192,2048]{1,0:T(8,128)(2,1)S(1)}, u32[]{:S(2)}, u32[]{:S(2)}) collective-permute-start(bf16[192,2048]{1,0:T(8,128)(2,1)S(1)} %get-tuple-element.19), channel_id=1, source_target_pairs={{16,8},{20,12},{24,16},{28,20},{17,9},{21,13},{25,17},{29,21},{18,... | collective-permute-start | bytes 2359304 | tf_op jit(solution)/shard_map/ppermute | solution.py:22
  180.2 18.8 %collective-permute-start.20 = (bf16[192,2048]{1,0:T(8,128)(2,1)S(1)}, bf16[192,2048]{1,0:T(8,128)(2,1)S(1)}, u32[]{:S(2)}, u32[]{:S(2)}) collective-permute-start(bf16[192,2048]{1,0:T(8,128)(2,1)S(1)} %get-tuple-element.20), channel_id=1, source_target_pairs={{0,8},{4,12},{8,16},{12,20},{1,9},{5,13},{9,17},{13,21},{2,10},{6,... | collective-permute-start | bytes 2359304 | tf_op jit(solution)/shard_map/ppermute | solution.py:22
  199.6 18.1 %collective-permute-start.18 = (bf16[192,2048]{1,0:T(8,128)(2,1)S(1)}, bf16[192,2048]{1,0:T(8,128)(2,1)S(1)}, u32[]{:S(2)}, u32[]{:S(2)}) collective-permute-start(bf16[192,2048]{1,0:T(8,128)(2,1)S(1)} %get-tuple-element.17), channel_id=1, source_target_pairs={{8,0},{12,4},{16,8},{20,12},{24,16},{28,20},{9,1},{13,5},{17,9},{2... | collective-permute-start | bytes 2359304 | tf_op jit(solution)/shard_map/ppermute | solution.py:22
  200.9 18.0 %collective-permute-start.21 = (bf16[192,2048]{1,0:T(8,128)(2,1)S(1)}, bf16[192,2048]{1,0:T(8,128)(2,1)S(1)}, u32[]{:S(2)}, u32[]{:S(2)}) collective-permute-start(bf16[192,2048]{1,0:T(8,128)(2,1)S(1)} %get-tuple-element.18), channel_id=1, source_target_pairs={{0,8},{4,12},{8,16},{12,20},{16,24},{20,28},{1,9},{5,13},{9,17},{1... | collective-permute-start | bytes 2359304 | tf_op jit(solution)/shard_map/ppermute | solution.py:22
  (15 other events, 148.3 us)
